TPU v7x, 512 devices: a whole 4x8x8 slice. The times are simulated.
512 devices in a mesh: kv: 64 (over z, y), tp: 8 (over x, core).
Axes of the slice: x: 4, y: 8, z: 8, core: 2. Of those that a mesh axis runs over, the one named last changes fastest.
Arguments:
- tokens: bfloat16 [8, 8192, 2048], P(None, 'kv'), may hold values from -32 to 32, as said below
- w_query: bfloat16 [2048, 1024], P(None, 'tp'), may hold values from -0.125 to 0.125
- w_key: bfloat16 [2048, 512], P(None, 'tp'), may hold values from -0.125 to 0.125
- w_value: bfloat16 [2048, 512], P(None, 'tp'), may hold values from -0.125 to 0.125
- w_output: bfloat16 [1024, 2048], P(None, 'tp'), may hold values from -3 to 3
- chosen: int32 [8, 64, 32], P(None, 'kv'), may hold values from -1 to 63, as said below
- lengths: int32 [8], replicated, may hold values from 1 to 8192, 22528 in all
Outputs:
- mixed: bfloat16 [8, 8192, 2048], P(None, 'kv', 'tp')
Inputs may be any that keep to these rules, and one draw needn't show every extreme that they name: chosen[s, b] lists distinct blocks of sequence s, none above b; its first entry is b; entries after the named ones are -1. For b >= 1 and each c < b, at most 4 of the 8 lists chosen[:, b] name block c, and exactly 4 of them name block b - 1. lengths[s] is the number of live positions of sequence s; the largest is 8192. `tokens`: activations of order one; some rows may be much larger.
All inputs are finite; a program needn't handle non-finite values.
Results may differ from a plain program's by a relative error of at most 0.012.
The roundings to bfloat16 on the way count: a program that leaves them out, or rounds other values in their place, can miss the bound.
Values may be sent and summed in bfloat16 or wider, within the bound.
A program may use at most 128 MiB of HBM per device.

v0:
```python
import jax
import jax.numpy as jnp
from jax import lax
from jax.sharding import PartitionSpec as P

HEADS = 16
KV_HEADS = 8
HEAD_DIM = 64


def per_device(tokens, w_query, w_key, w_value, w_output, chosen, lengths):
    seq_count, block_len, model_width = tokens.shape
    flat_rows = tokens.reshape(seq_count * block_len, model_width)
    queries = jnp.dot(flat_rows, w_query, preferred_element_type=jnp.float32).astype(jnp.bfloat16)
    key_proj = jnp.dot(flat_rows, w_key, preferred_element_type=jnp.float32).astype(jnp.bfloat16)
    value_proj = jnp.dot(flat_rows, w_value, preferred_element_type=jnp.float32).astype(
        jnp.bfloat16
    )
    key_width = key_proj.shape[1]
    local_blocks = jnp.concatenate([key_proj, value_proj], axis=1).reshape(
        seq_count, block_len, 2 * key_width
    )
    shard_member = lax.axis_index("kv")
    kv_devices = lax.axis_size("kv")
    picked = chosen[:, 0, :]
    clipped = jnp.maximum(picked, 0)
    seq_index = jnp.arange(seq_count, dtype=jnp.int32)
    gathered = lax.all_gather(local_blocks, "kv", axis=1, tiled=True)
    key_lookup = gathered.reshape(seq_count * kv_devices, block_len, 2 * key_width)
    source = seq_index[:, None] * kv_devices + clipped
    group_size = HEADS // KV_HEADS
    local_kv_heads = key_width // HEAD_DIM
    query_pos = shard_member * block_len + jnp.arange(block_len, dtype=jnp.int32)
    score_scale = HEAD_DIM ** (-0.5)

    def attend(packed):
        query_rows, source_row, pick_row, length = packed
        fetched = key_lookup[source_row]
        slot_count = pick_row.shape[0]
        key_rows = fetched[:, :, :key_width].reshape(
            slot_count * block_len, local_kv_heads, HEAD_DIM
        )
        value_rows = fetched[:, :, key_width:].reshape(
            slot_count * block_len, local_kv_heads, HEAD_DIM
        )
        grouped = query_rows.reshape(block_len, local_kv_heads, group_size, HEAD_DIM)
        scores = (
            jnp.einsum("qkgd,nkd->kgqn", grouped, key_rows, preferred_element_type=jnp.float32)
            * score_scale
        )
        key_pos = (
            pick_row[:, None] * block_len + jnp.arange(block_len, dtype=jnp.int32)[None, :]
        ).reshape(-1)
        listed = jnp.repeat(pick_row >= 0, block_len)
        allowed = (
            listed[None, :] & (key_pos[None, :] <= query_pos[:, None]) & (key_pos[None, :] < length)
        )
        masked = jnp.where(allowed, scores, -1e30)
        row_max = jnp.max(masked, axis=-1, keepdims=True)
        exponent = jnp.exp(masked - row_max)
        weights = (exponent / jnp.sum(exponent, axis=-1, keepdims=True)).astype(jnp.bfloat16)
        mixed_heads = jnp.einsum(
            "kgqn,nkd->qkgd", weights, value_rows, preferred_element_type=jnp.float32
        )
        live_rows = (query_pos < length)[:, None, None, None]
        return jnp.where(live_rows, mixed_heads, 0.0).astype(jnp.bfloat16).reshape(block_len, -1)

    attended = lax.map(attend, (queries.reshape(seq_count, block_len, -1), source, picked, lengths))
    attended_rows = attended.reshape(seq_count * block_len, -1)
    summed = jnp.dot(
        lax.all_gather(attended_rows, "tp", axis=1, tiled=True),
        w_output,
        preferred_element_type=jnp.float32,
    )
    return summed.astype(jnp.bfloat16).reshape(seq_count, block_len, -1)


def solution(mesh):
    return jax.shard_map(
        per_device,
        mesh=mesh,
        in_specs=(
            P(None, "kv", None),
            P(None, "tp"),
            P(None, "tp"),
            P(None, "tp"),
            P(None, "tp"),
            P(None, "kv", None),
            P(),
        ),
        out_specs=P(None, "kv", "tp"),
        check_vma=False,
    )
```

profile of v0, /device:TPU:1, one launch (start us, length us, event | category | flops | bytes accessed | tf_op | source)
XLA Modules:
  0.0 374.0 jit_solution(2250813190140114071)
XLA Ops:
  6.5 3.8 %convolution_convert_fusion.2 = bf16[1024,64]{0,1:T(8,128)(2,1)S(1)} fusion(bf16[1024,2048]{1,0:T(8,128)(2,1)} %bitcast.109, bf16[2048,64]{0,1:T(8,128)(2,1)} %param.12), kind=kOutput, calls=%fused_computation.31 | convolution fusion | flops 268500992 | bytes 4587520 | tf_op jit(solution)/shard_map/dot_general | solution.py:16
  12.7 4.2 %convolution_convert_fusion.1 = bf16[1024,128]{1,0:T(8,128)(2,1)} fusion(bf16[1024,2048]{1,0:T(8,128)(2,1)} %bitcast.110, bf16[2048,128]{1,0:T(8,128)(2,1)S(1)} %copy-done.5), kind=kOutput, calls=%fused_computation.30 | convolution fusion | flops 537001984 | bytes 4980736 | tf_op jit(solution)/shard_map/dot_general | solution.py:14
  16.9 144.8 %all-gather.3.cloned.1.call-done = bf16[8,8192,128]{1,0,2:T(8,128)(2,1)} async-done(((bf16[8,128,128]{1,0,2:T(8,128)(2,1)}), bf16[8,8192,128]{1,0,2:T(8,128)(2,1)}) %all-gather.3.cloned.1.call-update) | async-done | bytes 16777232 | tf_op jit(solution)/shard_map/all_gather | solution.py:28
  161.7 23.5 %copy.16 = bf16[8,8192,128]{2,1,0:T(8,128)(2,1)} copy(bf16[8,8192,128]{1,0,2:T(8,128)(2,1)} %all-gather.3.cloned.1.call-done) | data formatting | bytes 33554432 | tf_op jit(solution)/shard_map/all_gather | solution.py:28
  185.2 145.3 %while.11 = (s32[]{:T(128)}, bf16[8,128,128]{2,1,0:T(8,128)(2,1)S(1)}, s32[8]{0:T(128)S(1)}, s32[8,32]{1,0:T(8,128)S(1)}, bf16[512,128,128]{2,1,0:T(8,128)(2,1)}...) while((s32[]{:T(128)}, bf16[8,128,128]{2,1,0:T(8,128)(2,1)S(1)}, ...), condition=%wide.region_3.4_spmd.clone, body=%wide.region_0.3_spmd.clone.sunk | while | flops 278443040 | bytes 19263052 | solution.py:68
  186.7 3.5 and_and_fusion.2
  190.2 6.5 %gather_fusion = bf16[32,128,128]{2,1,0:T(8,128)(2,1)S(1)} fusion(bf16[512,128,128]{2,1,0:T(8,128)(2,1)} %get-tuple-element.182, s32[1024]{0:T(1024)S(1)} %pad_clamp_fusion.2), kind=kCustom, calls=%fused_computation.clone.clone.1 | custom fusion | bytes 2097280 | tf_op jit(solution)/shard_map/while/body/eval_jaxpr/gather | solution.py:38
  204.9 3.5 and_and_fusion.2
  208.4 6.5 %gather_fusion = bf16[32,128,128]{2,1,0:T(8,128)(2,1)S(1)} fusion(bf16[512,128,128]{2,1,0:T(8,128)(2,1)} %get-tuple-element.182, s32[1024]{0:T(1024)S(1)} %pad_clamp_fusion.2), kind=kCustom, calls=%fused_computation.clone.clone.1 | custom fusion | bytes 2097280 | tf_op jit(solution)/shard_map/while/body/eval_jaxpr/gather | solution.py:38
  223.0 3.5 and_and_fusion.2
  226.6 6.5 %gather_fusion = bf16[32,128,128]{2,1,0:T(8,128)(2,1)S(1)} fusion(bf16[512,128,128]{2,1,0:T(8,128)(2,1)} %get-tuple-element.182, s32[1024]{0:T(1024)S(1)} %pad_clamp_fusion.2), kind=kCustom, calls=%fused_computation.clone.clone.1 | custom fusion | bytes 2097280 | tf_op jit(solution)/shard_map/while/body/eval_jaxpr/gather | solution.py:38
  241.2 3.5 and_and_fusion.2
  244.7 6.5 %gather_fusion = bf16[32,128,128]{2,1,0:T(8,128)(2,1)S(1)} fusion(bf16[512,128,128]{2,1,0:T(8,128)(2,1)} %get-tuple-element.182, s32[1024]{0:T(1024)S(1)} %pad_clamp_fusion.2), kind=kCustom, calls=%fused_computation.clone.clone.1 | custom fusion | bytes 2097280 | tf_op jit(solution)/shard_map/while/body/eval_jaxpr/gather | solution.py:38
  253.6 2.1 fusion.46
  259.4 3.5 and_and_fusion.2
  262.9 6.5 %gather_fusion = bf16[32,128,128]{2,1,0:T(8,128)(2,1)S(1)} fusion(bf16[512,128,128]{2,1,0:T(8,128)(2,1)} %get-tuple-element.182, s32[1024]{0:T(1024)S(1)} %pad_clamp_fusion.2), kind=kCustom, calls=%fused_computation.clone.clone.1 | custom fusion | bytes 2097280 | tf_op jit(solution)/shard_map/while/body/eval_jaxpr/gather | solution.py:38
  277.5 3.5 and_and_fusion.2
  281.1 6.5 %gather_fusion = bf16[32,128,128]{2,1,0:T(8,128)(2,1)S(1)} fusion(bf16[512,128,128]{2,1,0:T(8,128)(2,1)} %get-tuple-element.182, s32[1024]{0:T(1024)S(1)} %pad_clamp_fusion.2), kind=kCustom, calls=%fused_computation.clone.clone.1 | custom fusion | bytes 2097280 | tf_op jit(solution)/shard_map/while/body/eval_jaxpr/gather | solution.py:38
  295.7 3.5 and_and_fusion.2
  299.2 6.5 %gather_fusion = bf16[32,128,128]{2,1,0:T(8,128)(2,1)S(1)} fusion(bf16[512,128,128]{2,1,0:T(8,128)(2,1)} %get-tuple-element.182, s32[1024]{0:T(1024)S(1)} %pad_clamp_fusion.2), kind=kCustom, calls=%fused_computation.clone.clone.1 | custom fusion | bytes 2097280 | tf_op jit(solution)/shard_map/while/body/eval_jaxpr/gather | solution.py:38
  313.9 3.5 and_and_fusion.2
  317.4 6.5 %gather_fusion = bf16[32,128,128]{2,1,0:T(8,128)(2,1)S(1)} fusion(bf16[512,128,128]{2,1,0:T(8,128)(2,1)} %get-tuple-element.182, s32[1024]{0:T(1024)S(1)} %pad_clamp_fusion.2), kind=kCustom, calls=%fused_computation.clone.clone.1 | custom fusion | bytes 2097280 | tf_op jit(solution)/shard_map/while/body/eval_jaxpr/gather | solution.py:38
  331.3 32.8 %all-gather.5.cloned.1.call-done = bf16[1024,1024]{1,0:T(8,128)(2,1)} async-done(((bf16[1024,128]{1,0:T(8,128)(2,1)}), bf16[1024,1024]{1,0:T(8,128)(2,1)}) %all-gather.5.cloned.1.call-update) | async-done | bytes 2097168 | tf_op jit(solution)/shard_map/all_gather | solution.py:71
  364.1 3.1 convolution_convert_fusion
  (167 shorter events, 65.7 us)
Async XLA Ops:
  6.5 357.5 %copy-start = (bf16[1024,256]{1,0:T(8,128)(2,1)S(1)}, bf16[1024,256]{1,0:T(8,128)(2,1)}, u32[]{:S(2)}) copy-start(bf16[1024,256]{1,0:T(8,128)(2,1)} %param.13) | copy-start | bytes 1572868
  6.5 3.8 %copy-start.2 = (bf16[2048,64]{0,1:T(8,128)(2,1)S(1)}, bf16[2048,64]{0,1:T(8,128)(2,1)}, u32[]{:S(2)}) copy-start(bf16[2048,64]{0,1:T(8,128)(2,1)} %param.11) | copy-start | bytes 786436
  6.5 155.2 %all-gather.3.cloned.1.call-start = ((), (), s32[]{:S(2)}) async-start(), calls=%async_computation | async-start | bytes 17039360 | tf_op jit(solution)/shard_map/all_gather | solution.py:28
  6.5 3.8 %copy-start.1 = (bf16[8,128,2048]{2,1,0:T(8,128)(2,1)S(1)}, bf16[8,128,2048]{2,1,0:T(8,128)(2,1)}, u32[]{:S(2)}) copy-start(bf16[8,128,2048]{2,1,0:T(8,128)(2,1)} %param.9) | copy-start | bytes 12582916
  10.3 2.3 copy-start.4
  10.3 2.4 copy-start.5
  12.5 351.5 %all-gather.5.cloned.1.call-start = ((), (), s32[]{:S(2)}) async-start(), calls=%async_computation.1 | async-start | bytes 2359296 | tf_op jit(solution)/shard_map/all_gather | solution.py:71
  16.9 168.4 %copy-start.6 = (s32[8]{0:T(128)S(1)}, s32[8]{0:T(128)}, u32[]{:S(2)}) copy-start(s32[8]{0:T(128)} %param.15) | copy-start | bytes 100
  330.6 0.7 copy-start.3
Sparse Core Ops, SparseCore 0:
  12.7 148.9 all-gather.2
  331.4 32.6 all-gather.4
where the time goes:
time: 376 us; the launch traced here: 374 us
  waiting for transfers between devices  178 us (47%)
  local copies, waits for them, and re-layouts  102 us (27%)
  other arithmetic  44.2 us (12%)
  matrix products  36 us (10%)
  between operations  13.5 us (4%)
    all_gather x1, waiting for transfers between devices, per_device(): gathered = lax.all_gather(local_blocks, 'kv', axis=1, tiled=True)  145 us
    gather x8, local copies, waits for them, and re-layouts, attend(): fetched = key_lookup[source_row]  52.1 us
    all_gather x1, waiting for transfers between devices, per_device(): lax.all_gather(attended_rows, 'tp', axis=1, tiled=True)  32.8 us
    and x8, other arithmetic, attend(): listed[None, :] & (key_pos[None, :] <= query_pos[:, None])  27.7 us
    all_gather x1, local copies, waits for them, and re-layouts, per_device(): gathered = lax.all_gather(local_blocks, 'kv', axis=1, tiled=True)  23.5 us
    dot_general x8, matrix products, attend(): jnp.einsum('qkgd,nkd->kgqn', grouped, key_rows, preferred_element_type=jn...  16.5 us
    dynamic_slice x24, local copies, waits for them, and re-layouts, per_device(): lax.map(attend, (queries.reshape(seq_count, block_len, -1), source, picke...  11.7 us
    slice x8, local copies, waits for them, and re-layouts, attend(): fetched[:, :, :key_width]  11.5 us
  transfers between devices with their start and end apart: 2, of which 2 were waited for; matrix products, arithmetic and copies ran while one was open for 1% of the time, Pallas kernels for 0%

commit v1 on v0

v1 whole, which is shorter than its diff:
```python
import functools

import jax
import jax.numpy as jnp
from jax import lax
from jax.experimental import pallas as pl
from jax.experimental.pallas import tpu as pltpu
from jax.sharding import PartitionSpec as P

SEQS = 8
BLK = 128
SEL = 32
HD = 64
MESH = pl.DeviceIdType.MESH
LOG2E = 1.4426950408889634
NEG = -1e30
RANKS = (8, 8, 7, 5, 4, 3, 3, 2)
UPTO = (2, 3, 5, 7, 7, 7, 7, 7)


def pick(table, index):
    value = jnp.int32(table[0])
    for i in range(1, len(table)):
        value = jnp.where(index == i, jnp.int32(table[i]), value)
    return value


def project_kernel(
    len_ref, chosen_ref, tok_ref, wq_ref, wk_ref, wv_ref,
    q_ref, kv_ref, bias_ref, meta_ref, tok_buf, w_buf, sems,
):
    block = lax.axis_index("kv")
    first = block * BLK
    for s in range(SEQS):
        rank = jnp.int32(0)
        for t in range(SEQS):
            if t != s:
                ahead = len_ref[t] > len_ref[s] if t > s else len_ref[t] >= len_ref[s]
                rank = rank + ahead.astype(jnp.int32)
        meta_ref[0, rank] = jnp.int32(s)
        meta_ref[1, rank] = len_ref[s]

    def fetch(r):
        return pltpu.make_async_copy(tok_ref.at[meta_ref[0, r]], tok_buf.at[r], sems.at[r])

    for r in range(SEQS):
        fetch(r).start()
    w_buf[:, 0:128] = wq_ref[...]
    w_buf[:, 128:256] = jnp.concatenate([wk_ref[...], wv_ref[...]], axis=1)

    def clear(i, carry):
        bias_ref[i // 64, i % 64] = jnp.float32(NEG)
        return carry

    lax.fori_loop(0, SEQS * 64, clear, 0)

    def mark(i, carry):
        r = i // SEL
        c = chosen_ref[meta_ref[0, r], i % SEL]

        @pl.when(c >= 0)
        def _():
            bias_ref[r, c] = jnp.float32(0.0)

        return carry

    lax.fori_loop(0, SEQS * SEL, mark, 0)
    lane = lax.broadcasted_iota(jnp.int32, (BLK, 128), 1)
    for g in range(SEQS // 2):
        for r in (2 * g, 2 * g + 1):
            fetch(r).wait()
        live = meta_ref[1, 2 * g] > first

        @pl.when(live)
        def _():
            rows = tok_buf[2 * g : 2 * g + 2].reshape(2 * BLK, -1)
            out = jnp.dot(rows, w_buf[...], preferred_element_type=jnp.float32)
            for i in range(2):
                part = out[i * BLK : (i + 1) * BLK]
                q = part[:, 0:128]
                q_ref[2 * g + i, 0:128] = jnp.where(lane < HD, q, 0.0).astype(jnp.bfloat16)
                q_ref[2 * g + i, 128:256] = jnp.where(
                    lane < HD, pltpu.roll(q, HD, 1), 0.0
                ).astype(jnp.bfloat16)
                kv_ref[2 * g + i] = part[:, 128:256].astype(jnp.bfloat16)

        @pl.when(jnp.logical_not(live))
        def _():
            q_ref[2 * g : 2 * g + 2] = jnp.zeros((2, 2 * BLK, 128), jnp.bfloat16)
            kv_ref[2 * g : 2 * g + 2] = jnp.zeros((2, BLK, 128), jnp.bfloat16)


def project(lengths, picked, tokens, w_query, w_key, w_value):
    smem = pl.BlockSpec(memory_space=pltpu.SMEM)
    vmem = pl.BlockSpec(memory_space=pltpu.VMEM)
    return pl.pallas_call(
        project_kernel,
        name="project",
        out_shape=(
            jax.ShapeDtypeStruct((SEQS, 2 * BLK, 128), jnp.bfloat16),
            jax.ShapeDtypeStruct((SEQS, BLK, 128), jnp.bfloat16),
            jax.ShapeDtypeStruct((SEQS, 64), jnp.float32),
            jax.ShapeDtypeStruct((2, SEQS), jnp.int32),
        ),
        in_specs=[smem, smem, pl.BlockSpec(memory_space=pl.ANY), vmem, vmem, vmem],
        out_specs=(vmem, vmem, smem, smem),
        scratch_shapes=[
            pltpu.VMEM((SEQS, BLK, 2048), jnp.bfloat16),
            pltpu.VMEM((2048, 256), jnp.bfloat16),
            pltpu.SemaphoreType.DMA((SEQS,)),
        ],
        compiler_params=pltpu.CompilerParams(vmem_limit_bytes=32 * 1024 * 1024),
    )(lengths, picked, tokens, w_query, w_key, w_value)


def exchange_kernel(
    ranks, bias_ref, meta_ref, q_ref, kv_ref, out_ref,
    buf, att, acc, top, own_sem, recv, send, ring_send, tp_recv, tp_send, out_sem,
):
    sizes = sorted(set(ranks))
    block = lax.axis_index("kv")
    member = lax.axis_index("tp")
    z, y = block // 8, lax.rem(block, 8)
    x, core = member // 2, lax.rem(member, 2)
    mine = pick(ranks, z)

    def at_kv(row, col):
        return {"kv": lax.rem(row + 8, 8) * 8 + lax.rem(col + 8, 8)}

    def at_tp(chip, which):
        return {"tp": lax.rem(chip + 4, 4) * 2 + which}

    own = pltpu.make_async_copy(kv_ref, buf.at[:, block], own_sem)
    own.start()
    barrier = pltpu.get_barrier_semaphore()

    def greet(target):
        pl.semaphore_signal(barrier, inc=1, device_id=target, device_id_type=MESH)

    for target in (
        at_kv(z, y + 1), at_kv(z, y - 1), at_kv(z + 1, y), at_kv(z - 1, y),
        at_tp(x + 1, core), at_tp(x - 1, core), at_tp(x, 1 - core),
    ):
        greet(target)

    @pl.when((z == 1) | (z == 2))
    def _():
        greet(at_kv(jnp.int32(7), y))

    @pl.when(z == 7)
    def _():
        greet(at_kv(jnp.int32(1), y))
        greet(at_kv(jnp.int32(2), y))

    extra = jnp.where((z == 1) | (z == 2), 1, jnp.where(z == 7, 2, 0))
    pl.semaphore_wait(barrier, 7 + extra)
    own.wait()

    def each_size(size, act):
        for k in sizes:
            @pl.when(size == k)
            def _(k=k):
                act(k)

    def link(c, k, sem, target):
        part = buf.at[0:k, c]
        return pltpu.make_async_remote_copy(
            src_ref=part, dst_ref=part, send_sem=sem, recv_sem=recv.at[c],
            device_id=target, device_id_type=MESH,
        )

    def start(c, size, sem, target):
        each_size(size, lambda k: link(c, k, sem, target).start())

    def sent(c, size, sem):
        each_size(size, lambda k: link(c, k, sem, at_kv(z, y + 1)).wait_send())

    def arrived(c, size):
        each_size(size, lambda k: link(c, k, send.at[0, c], at_kv(z, y + 1)).wait_recv())

    def route(row):
        upto = pick(UPTO, row)
        rises = z <= upto
        hops = jnp.where(rises, z - row, 8 - z)
        last_size = pick(ranks, jnp.minimum(upto + 1, 7))
        size_in = jnp.where(rises, mine, last_size)
        up = rises & (z < upto)
        wrap = (z == row) & (upto < 7)
        down = jnp.logical_not(rises) & (z > upto + 1)
        return upto, hops, last_size, size_in, up, wrap, down

    up_size = pick(ranks, jnp.minimum(z + 1, 7))

    def column(act, row, c):
        _, _, last_size, _, up, wrap, down = route(row)

        @pl.when(up)
        def _():
            act(c, up_size, send.at[0, c], at_kv(z + 1, y))

        @pl.when(wrap)
        def _():
            act(c, last_size, send.at[1, c], at_kv(jnp.int32(7), y))

        @pl.when(down)
        def _():
            act(c, last_size, send.at[1, c], at_kv(z - 1, y))

    def left_of(step):
        return lax.rem(y - step + 8, 8)

    def right_of(step):
        return lax.rem(y + step, 8)

    def row_item(act, await_it, row, j):
        step = (j + 1) // 2
        from_left = lax.rem(j, 2) == 1
        c = row * 8 + jnp.where(from_left, left_of(step), right_of(step))
        in_row = row == z
        if await_it:
            _, _, _, size_in, _, _, _ = route(row)

            @pl.when(jnp.logical_not(in_row & (j == 0)))
            def _():
                arrived(c, size_in)

        @pl.when(in_row & ((j == 0) | (from_left & (step < 4))))
        def _():
            act(c, mine, ring_send.at[0, c], at_kv(z, y + 1))

        @pl.when(in_row & (jnp.logical_not(from_left) & (step < 3)))
        def _():
            act(c, mine, ring_send.at[1, c], at_kv(z, y - 1))

        column(act, row, c)

    def column_item(act, await_it, row, step):
        @pl.when(step == 0)
        def _():
            c = row * 8 + y
            if await_it:
                _, _, _, size_in, _, _, _ = route(row)

                @pl.when(row != z)
                def _():
                    arrived(c, size_in)

            act(c, mine, ring_send.at[0, c], at_kv(z, y + 1))
            act(c, mine, ring_send.at[1, c], at_kv(z, y - 1))
            column(act, row, c)

        @pl.when(step > 0)
        def _():
            c = row * 8 + left_of(step)
            if await_it:
                arrived(c, mine)

            @pl.when(step < 4)
            def _():
                act(c, mine, ring_send.at[0, c], at_kv(z, y + 1))

        @pl.when((step > 0) & (step < 4))
        def _():
            c = row * 8 + right_of(step)
            if await_it:
                arrived(c, mine)

            @pl.when(step < 3)
            def _():
                act(c, mine, ring_send.at[1, c], at_kv(z, y - 1))

    def waves(item, items, waves_count):
        def wave(t, carry):
            def one(row, carry):
                _, hops, _, _, _, _, _ = route(row)
                j = t - hops

                @pl.when((j >= 0) & (j < items))
                def _():
                    item(start, True, row, j)

                return carry

            return lax.fori_loop(0, z + 1, one, carry)

        lax.fori_loop(0, waves_count, wave, 0)

    def drain(item, items):
        def one(i, carry):
            item(lambda c, size, sem, target: sent(c, size, sem), False, i // items, lax.rem(i, items))
            return carry

        lax.fori_loop(0, (z + 1) * items, one, 0)

    @pl.when(core == 0)
    def _():
        waves(row_item, 8, 13)

    @pl.when(core == 1)
    def _():
        waves(column_item, 5, 10)

    scale = HD ** (-0.5) * LOG2E
    row_at = lax.rem(lax.broadcasted_iota(jnp.int32, (2 * BLK, BLK), 0), BLK)
    col_at = lax.broadcasted_iota(jnp.int32, (2 * BLK, BLK), 1)
    ones = jnp.ones((8 * BLK, BLK), jnp.bfloat16)
    lane = lax.broadcasted_iota(jnp.int32, (BLK, BLK), 1)
    sub = lax.broadcasted_iota(jnp.int32, (BLK, BLK), 0)

    def scores(r, row, diagonal):
        keys = buf[r, pl.ds(row * 8, 8)].reshape(8 * BLK, BLK)
        raw = lax.dot_general(
            q_ref[r], keys, (((1,), (1,)), ((), ())), preferred_element_type=jnp.float32
        )
        parts = []
        for i in range(8):
            part = raw[:, i * BLK : (i + 1) * BLK] * scale + bias_ref[r, row * 8 + i]
            if diagonal:
                part = jnp.where((col_at <= row_at) | (y != i), part, NEG)
            parts.append(part)
        return jnp.concatenate(parts, axis=1), jnp.concatenate([keys, ones], axis=1)

    def one_rank(r, carry):
        s, wide = scores(r, z, True)
        best = jnp.max(s, axis=1, keepdims=True)
        p = jnp.exp2(s - best).astype(jnp.bfloat16)
        top[...] = best
        acc[...] = jnp.dot(p, wide, preferred_element_type=jnp.float32)

        def one_row(i, carry):
            s, wide = scores(r, z - 1 - i, False)
            old = top[...]
            best = jnp.maximum(old, jnp.max(s, axis=1, keepdims=True))
            p = jnp.exp2(s - best).astype(jnp.bfloat16)
            top[...] = best
            acc[...] = acc[...] * jnp.exp2(old - best) + jnp.dot(
                p, wide, preferred_element_type=jnp.float32
            )
            return carry

        lax.fori_loop(0, z, one_row, 0)
        full = acc[:, 0:128] / acc[:, 128:256]
        both = jnp.where(lane < HD, pltpu.roll(full[0:BLK], HD, 1), full[BLK:])
        both = jnp.where(sub + block * BLK < meta_ref[1, r], both, 0.0)
        att[r, :, pl.ds(pl.multiple_of(member * BLK, BLK), BLK)] = both.astype(jnp.bfloat16)
        return carry

    lax.fori_loop(0, mine, one_rank, 0)

    def share(chip, which, k, half, slot, target):
        lo, hi = {0: (0, k), 1: (0, k // 2), 2: (k // 2, k)}[half]
        t = lax.rem(chip + 4, 4) * 2 + which
        part = att.at[lo:hi, :, pl.ds(pl.multiple_of(t * BLK, BLK), BLK)]
        return pltpu.make_async_remote_copy(
            src_ref=part, dst_ref=part, send_sem=tp_send.at[slot], recv_sem=tp_recv.at[slot],
            device_id=target, device_id_type=MESH,
        )

    right, left, sibling = at_tp(x + 1, core), at_tp(x - 1, core), at_tp(x, 1 - core)

    def tp_steps(k):
        def go(chip, half, slot, target):
            if half == 1 and k < 2:
                return
            share(chip, core, k, half, slot, target).start()

        def got(chip, which, half, slot):
            if half == 1 and k < 2:
                return
            share(chip, which, k, half, slot, right).wait_recv()

        def done(half, slot):
            if half == 1 and k < 2:
                return
            share(x, core, k, half, slot, right).wait_send()

        go(x, 0, 0, right)
        go(x, 0, 1, left)
        go(x, 0, 2, sibling)
        got(x - 1, core, 0, 0)
        go(x - 1, 1, 3, right)
        go(x - 1, 0, 5, sibling)
        got(x + 1, core, 0, 1)
        go(x + 1, 2, 4, left)
        go(x + 1, 0, 6, sibling)
        got(x - 2, core, 1, 3)
        go(x - 2, 1, 7, sibling)
        got(x + 2, core, 2, 4)
        go(x + 2, 2, 8, sibling)
        got(x, 1 - core, 0, 2)
        got(x - 1, 1 - core, 0, 5)
        got(x + 1, 1 - core, 0, 6)
        got(x - 2, 1 - core, 1, 7)
        got(x + 2, 1 - core, 2, 8)
        for half, slot in ((0, 0), (0, 1), (0, 2), (1, 3), (2, 4), (0, 5), (0, 6), (1, 7), (2, 8)):
            done(half, slot)

    each_size(mine, tp_steps)

    @pl.when(core == 0)
    def _():
        drain(row_item, 8)

    @pl.when(core == 1)
    def _():
        drain(column_item, 5)

    result = pltpu.make_async_copy(att, out_ref, out_sem)
    result.start()
    result.wait()


def exchange(bias, meta, queries, keyvals):
    smem = pl.BlockSpec(memory_space=pltpu.SMEM)
    vmem = pl.BlockSpec(memory_space=pltpu.VMEM)
    return pl.pallas_call(
        functools.partial(exchange_kernel, RANKS),
        name="exchange",
        out_shape=jax.ShapeDtypeStruct((SEQS, BLK, 1024), jnp.bfloat16),
        in_specs=[smem, smem, vmem, vmem],
        out_specs=pl.BlockSpec(memory_space=pl.ANY),
        scratch_shapes=[
            pltpu.VMEM((SEQS, 64, BLK, BLK), jnp.bfloat16),
            pltpu.VMEM((SEQS, BLK, 1024), jnp.bfloat16),
            pltpu.VMEM((2 * BLK, 2 * BLK), jnp.float32),
            pltpu.VMEM((2 * BLK, 1), jnp.float32),
            pltpu.SemaphoreType.DMA,
            pltpu.SemaphoreType.DMA((64,)),
            pltpu.SemaphoreType.DMA((2, 64)),
            pltpu.SemaphoreType.DMA((2, 64)),
            pltpu.SemaphoreType.DMA((9,)),
            pltpu.SemaphoreType.DMA((9,)),
            pltpu.SemaphoreType.DMA,
        ],
        compiler_params=pltpu.CompilerParams(
            collective_id=0, has_side_effects=True, vmem_limit_bytes=48 * 1024 * 1024
        ),
    )(bias, meta, queries, keyvals)


def finish_kernel(meta_ref, att_ref, w_ref, out_ref, att_buf, sems):
    first = lax.axis_index("kv") * BLK

    def fetch(r):
        return pltpu.make_async_copy(att_ref.at[r], att_buf.at[r], sems.at[r])

    for r in range(SEQS):
        fetch(r).start()
    for r in range(SEQS):
        fetch(r).wait()
        s = meta_ref[0, r]
        live = meta_ref[1, r] > first

        @pl.when(live)
        def _():
            out_ref[s] = jnp.dot(
                att_buf[r], w_ref[...], preferred_element_type=jnp.float32
            ).astype(jnp.bfloat16)

        @pl.when(jnp.logical_not(live))
        def _():
            out_ref[s] = jnp.zeros((BLK, 256), jnp.bfloat16)


def finish(meta, attended, w_output):
    vmem = pl.BlockSpec(memory_space=pltpu.VMEM)
    return pl.pallas_call(
        finish_kernel,
        name="finish",
        out_shape=jax.ShapeDtypeStruct((SEQS, BLK, 256), jnp.bfloat16),
        in_specs=[pl.BlockSpec(memory_space=pltpu.SMEM), pl.BlockSpec(memory_space=pl.ANY), vmem],
        out_specs=vmem,
        scratch_shapes=[
            pltpu.VMEM((SEQS, BLK, 1024), jnp.bfloat16),
            pltpu.SemaphoreType.DMA((SEQS,)),
        ],
        compiler_params=pltpu.CompilerParams(vmem_limit_bytes=16 * 1024 * 1024),
    )(meta, attended, w_output)


def per_device(tokens, w_query, w_key, w_value, w_output, chosen, lengths):
    queries, keyvals, bias, meta = project(
        lengths, chosen[:, 0, :], tokens, w_query, w_key, w_value
    )
    attended = exchange(bias, meta, queries, keyvals)
    return finish(meta, attended, w_output)


def solution(mesh):
    return jax.shard_map(
        per_device,
        mesh=mesh,
        in_specs=(
            P(None, "kv", None),
            P(None, "tp"),
            P(None, "tp"),
            P(None, "tp"),
            P(None, "tp"),
            P(None, "kv", None),
            P(),
        ),
        out_specs=P(None, "kv", "tp"),
        check_vma=False,
    )
```

time: 376 us -> 126 us (0.34)
  the two profiles are of different devices: /device:TPU:1 before, /device:TPU:193 now
where the time goes in v1:
time: 126 us; the launch traced here: 125 us
  Pallas kernels  118 us (94%)
  local copies, waits for them, and re-layouts  7.02 us (6%)
    pallas_call x1, Pallas kernels, exchange(): pl.pallas_call(functools.partial(exchange_kernel, RANKS), name='exchange'...  103 us
    pallas_call x1, Pallas kernels, project(): pl.pallas_call(project_kernel, name='project', out_shape=(jax.ShapeDtypeS...  12.7 us
    unnamed x12, local copies, waits for them, and re-layouts  7.02 us

profile of v1, /device:TPU:193, one launch (start us, length us, event | category | flops | bytes accessed | tf_op | source)
XLA Modules:
  0.0 125.3 jit_solution(13310018577039405008)
XLA Ops:
  0.0 1.2 copy.8.wk_ref
  1.2 1.2 copy.9.wv_ref
  2.5 0.0 copy-start
  2.5 2.2 %copy-done = bf16[8,128,2048]{2,1,0:T(8,128)(2,1)S(1)} copy-done((bf16[8,128,2048]{2,1,0:T(8,128)(2,1)S(1)}, bf16[8,128,2048]{2,1,0:T(8,128)(2,1)}, u32[]{:S(2)}) %copy-start) | copy-done | bytes 4194328
  4.7 0.0 copy-start.2
  4.7 1.0 copy-done.2
  5.7 0.0 copy-start.3
  5.7 0.7 copy-done.3
  6.4 0.0 copy-start.4
  6.4 0.7 copy-done.4
  7.0 0.0 copy-start.1
  7.0 12.7 %project.1 = (bf16[8,256,128]{2,1,0:T(8,128)(2,1)S(1)}, bf16[8,128,128]{2,1,0:T(8,128)(2,1)S(1)}, f32[8,64]{1,0:T(8,128)S(1)}, s32[2,8]{1,0:T(2,128)S(1)}) custom-call(s32[8]{0:T(128)S(1)} %copy-done.4, s32[8,32]{1,0:T(8,128)S(1)} %bitcast.1, bf16[8,128,2048]{2,1,0:T(8,128)(2,1)S(1)} %copy-done, bf16[2048,128]{1,0:T(8,128)(2,1)S(1)} %copy-done.2, ...), custom_call_target="tpu_custom_call" | custom-call | tf_op jit(solution)/shard_map/project/pallas_call | solution.py:96
  19.8 103.3 %exchange.1.att_ref = bf16[8,128,1024]{2,1,0:T(8,128)(2,1)S(1)} custom-call(f32[8,64]{1,0:T(8,128)S(1)} %get-tuple-element.10.bias_ref, s32[2,8]{1,0:T(2,128)S(1)} %get-tuple-element.9.meta_ref, bf16[8,256,128]{2,1,0:T(8,128)(2,1)S(1)} %get-tuple-element.11.q_ref, bf16[8,128,128]{2,1,0:T(8,128)(2,1)S(1)} %get-tuple-element.12.kv_ref), custom_call_target="tpu_custom_call" | custom-call | tf_op jit(solution)/shard_map/exchange/pallas_call | solution.py:416
  123.1 0.0 copy-done.1
  123.1 2.1 %finish.1 = bf16[8,128,256]{2,1,0:T(8,128)(2,1)} custom-call(s32[2,8]{1,0:T(2,128)S(1)} %get-tuple-element.9.meta_ref, bf16[8,128,1024]{2,1,0:T(8,128)(2,1)S(1)} %exchange.1.att_ref, bf16[1024,256]{1,0:T(8,128)(2,1)S(1)} %copy-done.1), custom_call_target="tpu_custom_call" | custom-call | tf_op jit(solution)/shard_map/finish/pallas_call | solution.py:467
Async XLA Ops:
  2.5 2.2 %copy-start = (bf16[8,128,2048]{2,1,0:T(8,128)(2,1)S(1)}, bf16[8,128,2048]{2,1,0:T(8,128)(2,1)}, u32[]{:S(2)}) copy-start(bf16[8,128,2048]{2,1,0:T(8,128)(2,1)} %tok_ref.1) | copy-start | bytes 12582916
  4.7 1.0 copy-start.2
  5.7 0.7 copy-start.3
  6.4 0.7 copy-start.4
  7.0 116.1 %copy-start.1 = (bf16[1024,256]{1,0:T(8,128)(2,1)S(1)}, bf16[1024,256]{1,0:T(8,128)(2,1)}, u32[]{:S(2)}) copy-start(bf16[1024,256]{1,0:T(8,128)(2,1)} %w_ref.1) | copy-start | bytes 1572868

commit v2 on v0

v2 whole, which is shorter than its diff:
```python
import functools

import jax
import jax.numpy as jnp
from jax import lax
from jax.experimental import pallas as pl
from jax.experimental.pallas import tpu as pltpu
from jax.sharding import PartitionSpec as P

SEQS = 8
BLK = 128
SEL = 32
HD = 64
MESH = pl.DeviceIdType.MESH
LOG2E = 1.4426950408889634
NEG = -1e30
GROUPS = ((0, 2), (2, 2), (4, 1), (5, 3))
SKEW = (0, 0, 1, 1)
UPTO = (3, 4, 5, 7, 7, 7, 7, 7)
FULL = ((8, 8, 7, 5, 4, 3, 3, 2), (8, 7, 4, 3))
LIGHT = ((8, 8, 5, 4, 2, 2, 2, 1), (8, 4, 3, 2))


def project_kernel(
    len_ref, chosen_ref, tok_ref, wq_ref, wk_ref, wv_ref,
    q_ref, kv_ref, bias_ref, meta_ref, tok_buf, w_buf, wt_buf, row_buf, sems, w_sems,
):
    block = lax.axis_index("kv")
    first = block * BLK
    weights = (
        pltpu.make_async_copy(wk_ref, wt_buf.at[0:HD], w_sems.at[0]),
        pltpu.make_async_copy(wv_ref, wt_buf.at[HD : 2 * HD], w_sems.at[1]),
        pltpu.make_async_copy(wq_ref, w_buf.at[:, 0:128], w_sems.at[2]),
    )
    for copy in weights:
        copy.start()
    for s in range(SEQS):
        rank = jnp.int32(0)
        for t in range(SEQS):
            if t != s:
                ahead = len_ref[t] > len_ref[s] if t > s else len_ref[t] >= len_ref[s]
                rank = rank + ahead.astype(jnp.int32)
        meta_ref[0, rank] = jnp.int32(s)
        meta_ref[1, rank] = len_ref[s]
    light = jnp.int32(1)
    for row, most in enumerate(LIGHT[0]):
        if most < SEQS:
            light = jnp.where(meta_ref[1, most] > 8 * BLK * row, 0, light)
    for i in range(SEQS):
        meta_ref[2, i] = light

    def fetch(r):
        return pltpu.make_async_copy(tok_ref.at[meta_ref[0, r]], tok_buf.at[r], sems.at[r])

    for r in range(SEQS):
        fetch(r).start()
    for r in range(SEQS):
        row_buf[r : r + 1] = chosen_ref[pl.ds(meta_ref[0, r], 1)]
    picked = row_buf[...]
    for c in range(64):
        listed = jnp.max(jnp.where(picked == c, 0.0, NEG), axis=1, keepdims=True)
        bias_ref[:, c * BLK : (c + 1) * BLK] = jnp.broadcast_to(listed, (SEQS, BLK))
    weights[0].wait()
    weights[1].wait()
    w_buf[:, 128:256] = wt_buf[...].T
    weights[2].wait()
    lane = lax.broadcasted_iota(jnp.int32, (BLK, 128), 1)
    for g in range(SEQS // 2):
        for r in (2 * g, 2 * g + 1):
            fetch(r).wait()
        live = meta_ref[1, 2 * g] > first

        @pl.when(live)
        def _():
            rows = tok_buf[2 * g : 2 * g + 2].reshape(2 * BLK, -1)
            out = jnp.dot(rows, w_buf[...], preferred_element_type=jnp.float32)
            for i in range(2):
                part = out[i * BLK : (i + 1) * BLK]
                q = part[:, 0:128]
                q_ref[2 * g + i, 0:128] = jnp.where(lane < HD, q, 0.0).astype(jnp.bfloat16)
                q_ref[2 * g + i, 128:256] = jnp.where(
                    lane < HD, pltpu.roll(q, HD, 1), 0.0
                ).astype(jnp.bfloat16)
                kv_ref[2 * g + i] = part[:, 128:256].astype(jnp.bfloat16)

        @pl.when(jnp.logical_not(live))
        def _():
            q_ref[2 * g : 2 * g + 2] = jnp.zeros((2, 2 * BLK, 128), jnp.bfloat16)
            kv_ref[2 * g : 2 * g + 2] = jnp.zeros((2, BLK, 128), jnp.bfloat16)


def project(lengths, picked, tokens, w_query, w_key, w_value):
    smem = pl.BlockSpec(memory_space=pltpu.SMEM)
    vmem = pl.BlockSpec(memory_space=pltpu.VMEM)
    hbm = pl.BlockSpec(memory_space=pltpu.HBM)
    return pl.pallas_call(
        project_kernel,
        name="project",
        out_shape=(
            jax.ShapeDtypeStruct((SEQS, 2 * BLK, 128), jnp.bfloat16),
            jax.ShapeDtypeStruct((SEQS, BLK, 128), jnp.bfloat16),
            jax.ShapeDtypeStruct((SEQS, 64 * BLK), jnp.float32),
            jax.ShapeDtypeStruct((3, SEQS), jnp.int32),
        ),
        in_specs=[smem, vmem, hbm, hbm, hbm, hbm],
        out_specs=(vmem, vmem, vmem, smem),
        scratch_shapes=[
            pltpu.VMEM((SEQS, BLK, 2048), jnp.bfloat16),
            pltpu.VMEM((2048, 256), jnp.bfloat16),
            pltpu.VMEM((2 * HD, 2048), jnp.bfloat16),
            pltpu.VMEM((SEQS, SEL), jnp.int32),
            pltpu.SemaphoreType.DMA((SEQS,)),
            pltpu.SemaphoreType.DMA((3,)),
        ],
    )(lengths, picked, tokens, w_query, w_key.T, w_value.T)


def nibble(table):
    packed = sum(v << (4 * i) for i, v in enumerate(table))

    def look(index):
        return (jnp.int32(packed) >> (4 * index)) & 15

    return look


def hop_count(at, row):
    return at - row if at <= UPTO[row] else 8 - at


def exchange_kernel(
    plan, bias_ref, meta_ref, q_ref, kv_ref, att,
    buf, acc, top, own_sem, recv, send, tp_recv, tp_send,
):
    ranks, reach = plan
    ranks_at, upto_at = nibble(ranks), nibble(UPTO)
    hops_max_at = nibble([max(hop_count(at, row) for row in range(at + 1)) for at in range(8)])
    block = lax.axis_index("kv")
    member = lax.axis_index("tp")
    z, y = block >> 3, block & 7
    x, core = member >> 1, member & 1
    mine = ranks_at(z)
    first_core = core == 0

    def at_kv(row, col):
        return {"kv": (row & 7) * 8 + (col & 7)}

    def at_tp(chip, which):
        return {"tp": (chip & 3) * 2 + which}

    own = pltpu.make_async_copy(kv_ref, buf.at[:, block], own_sem)
    own.start()
    barrier = pltpu.get_barrier_semaphore()

    def greet(target):
        pl.semaphore_signal(barrier, inc=1, device_id=target, device_id_type=MESH)

    for target in (
        at_kv(z, y + 1), at_kv(z, y - 1),
        at_tp(x + 1, core), at_tp(x - 1, core), at_tp(x, 1 - core),
    ):
        greet(target)
    for step in (1, 2, 6, 7):
        greet(at_kv(z + step, y))

    @pl.when(z == 2)
    def _():
        greet(at_kv(jnp.int32(7), y))

    @pl.when(z == 7)
    def _():
        greet(at_kv(jnp.int32(2), y))

    pl.semaphore_wait(barrier, jnp.where((z == 2) | (z == 7), 10, 9))
    own.wait()

    def link(g, c, sem, target):
        lo, count = GROUPS[g]
        part = buf.at[lo : lo + count, c]
        return pltpu.make_async_remote_copy(
            src_ref=part, dst_ref=part, send_sem=sem, recv_sem=recv.at[g, c],
            device_id=target, device_id_type=MESH,
        )

    def to_right(g, c, row):
        link(g, c, send.at[0, g, row], at_kv(z, y + 1)).start()

    def to_left(g, c, row):
        link(g, c, send.at[1, g, row], at_kv(z, y - 1)).start()

    def arrived(g, c):
        link(g, c, send.at[0, 0, 0], at_kv(z, y + 1)).wait_recv()

    def route(row):
        upto = upto_at(row)
        rises = z <= upto
        hops = jnp.where(rises, z - row, 8 - z)
        return upto, rises, hops

    def needs(g, row, upto, rises):
        up = rises & (z < jnp.minimum(upto, reach[g] - 1))
        falls = upto + 1 < reach[g]
        wrap = (z == row) & falls
        down = jnp.logical_not(rises) & (z > upto + 1) & falls
        takes = (rises & (z < reach[g])) | (jnp.logical_not(rises) & falls)
        return takes, up, wrap, down

    def column(g, c, row, up, wrap, down):
        @pl.when(up)
        def _():
            link(g, c, send.at[2, g, row], at_kv(z + 1, y)).start()

        @pl.when(wrap)
        def _():
            link(g, c, send.at[3, g, row], at_kv(jnp.int32(7), y)).start()

        @pl.when(down)
        def _():
            link(g, c, send.at[3, g, row], at_kv(z - 1, y)).start()

    def row_items(u, row, upto, rises):
        for g in range(len(GROUPS)):
            step = u - SKEW[g]
            takes, up, wrap, down = needs(g, row, upto, rises)
            in_row = row == z

            @pl.when((step >= 0) & (step < 5) & takes)
            def _(g=g, step=step, up=up, wrap=wrap, down=down, in_row=in_row):
                c = row * 8 + ((y - step) & 7)

                @pl.when(jnp.logical_not(in_row & (step == 0)))
                def _():
                    arrived(g, c)

                @pl.when(in_row & (step < 4))
                def _():
                    to_right(g, c, row)

                @pl.when(in_row & (step == 0))
                def _():
                    to_left(g, c, row)

                column(g, c, row, up, wrap, down)

                @pl.when((step > 0) & (step < 4))
                def _():
                    c = row * 8 + ((y + step) & 7)
                    arrived(g, c)

                    @pl.when(in_row & (step < 3))
                    def _():
                        to_left(g, c, row)

                    column(g, c, row, up, wrap, down)

    def column_items(t, row):
        away = z - row
        far = (away + 1) >> 1
        for g in range(len(GROUPS)):
            step = t - far - SKEW[g]
            used = z < reach[g]

            @pl.when((step == 0) & used)
            def _(g=g):
                c = row * 8 + y

                @pl.when(row != z)
                def _():
                    arrived(g, c)

                to_right(g, c, row)
                to_left(g, c, row)

                for ahead in (1, 2):
                    @pl.when(((away & 1) == 0) & (z + ahead < reach[g]))
                    def _(ahead=ahead):
                        link(g, c, send.at[1 + ahead, g, row], at_kv(z + ahead, y)).start()

            @pl.when((step > 0) & (step < 5) & used)
            def _(g=g, step=step):
                c = row * 8 + ((y - step) & 7)
                arrived(g, c)

                @pl.when(step < 4)
                def _():
                    to_right(g, c, row)
                    c2 = row * 8 + ((y + step) & 7)
                    arrived(g, c2)

                    @pl.when(step < 3)
                    def _():
                        to_left(g, c2, row)

    scale = HD ** (-0.5) * LOG2E
    row_at = lax.broadcasted_iota(jnp.int32, (2 * BLK, BLK), 0) & (BLK - 1)
    col_at = lax.broadcasted_iota(jnp.int32, (2 * BLK, BLK), 1)
    ones = jnp.ones((8 * BLK, BLK), jnp.bfloat16)
    lane = lax.broadcasted_iota(jnp.int32, (BLK, BLK), 1)
    sub = lax.broadcasted_iota(jnp.int32, (BLK, BLK), 0)

    def scores(r, row):
        keys = buf[r, pl.ds(row * 8, 8)].reshape(8 * BLK, BLK)
        raw = lax.dot_general(
            q_ref[r], keys, (((1,), (1,)), ((), ())), preferred_element_type=jnp.float32
        )
        bias = bias_ref[pl.ds(r, 1), pl.ds(pl.multiple_of(row * 8 * BLK, 8 * BLK), 8 * BLK)]
        return raw * scale + bias, jnp.concatenate([keys, ones], axis=1)

    def attend(r, row):
        @pl.when(row == z)
        def _():
            s, wide = scores(r, row)
            parts = []
            for i in range(8):
                part = s[:, i * BLK : (i + 1) * BLK]
                parts.append(jnp.where((col_at <= row_at) | (y != i), part, NEG))
            s = jnp.concatenate(parts, axis=1)
            best = jnp.max(s, axis=1, keepdims=True)
            p = jnp.exp2(s - best).astype(jnp.bfloat16)
            top[r] = best
            acc[r] = jnp.dot(p, wide, preferred_element_type=jnp.float32)

        @pl.when(row != z)
        def _():
            s, wide = scores(r, row)
            old = top[r]
            best = jnp.maximum(old, jnp.max(s, axis=1, keepdims=True))
            p = jnp.exp2(s - best).astype(jnp.bfloat16)
            top[r] = best
            acc[r] = acc[r] * jnp.exp2(old - best) + jnp.dot(
                p, wide, preferred_element_type=jnp.float32
            )

    def settle(r):
        total = acc[r]
        full = total[:, 0:128] / total[:, 128:256]
        both = jnp.where(lane < HD, pltpu.roll(full[0:BLK], HD, 1), full[BLK:])
        both = jnp.where(sub + block * BLK < meta_ref[1, r], both, 0.0)
        att[member, r] = both.astype(jnp.bfloat16)

    def share(g, chip, which, slot, target):
        t = (chip & 3) * 2 + which
        lo, count = GROUPS[g]
        part = att.at[t, lo : lo + count]
        return pltpu.make_async_remote_copy(
            src_ref=part, dst_ref=part, send_sem=tp_send.at[g, slot], recv_sem=tp_recv.at[g, slot],
            device_id=target, device_id_type=MESH,
        )

    right, left, sibling = at_tp(x + 1, core), at_tp(x - 1, core), at_tp(x, 1 - core)

    def share_own(g):
        share(g, x, core, 0, right).start()
        share(g, x, core, 1, left).start()
        share(g, x, core, 2, sibling).start()

    def share_next(g):
        share(g, x - 1, core, 0, right).wait_recv()
        if g % 2 == 0:
            share(g, x - 1, core, 3, right).start()
        share(g, x - 1, core, 4, sibling).start()
        share(g, x + 1, core, 1, right).wait_recv()
        if g % 2 == 1:
            share(g, x + 1, core, 3, left).start()
        share(g, x + 1, core, 5, sibling).start()

    def share_far(g):
        share(g, x + 2, core, 3, right).wait_recv()
        share(g, x + 2, core, 6, sibling).start()

    last = len(GROUPS) - 1
    farthest = jnp.where(first_core, hops_max_at(z), (z + 1) >> 1)

    def delay_of(row):
        return jnp.where(first_core, route(row)[2], (z - row + 1) >> 1)


    def wave(t, carry):
        def comm(i, carry):
            row = z - i
            upto, rises, hops = route(row)
            u = t - hops

            @pl.when(first_core)
            def _():
                row_items(u, row, upto, rises)

            @pl.when(jnp.logical_not(first_core))
            def _():
                column_items(t, row)

            return carry

        lax.fori_loop(0, z + 1, comm, 0)

        def matching(at):
            lo, hi = jnp.int32(8), jnp.int32(0)
            for g, (first, count) in enumerate(GROUPS):
                hit = at == SKEW[g] + 4
                lo = jnp.where(hit, jnp.minimum(lo, first), lo)
                hi = jnp.where(hit, jnp.maximum(hi, first + count), hi)
            return lo, jnp.minimum(hi, mine)

        def compute(i, carry):
            row = z - i
            lo, hi = matching(t - delay_of(row))

            def one(r, carry):
                attend(r, row)
                return carry

            @pl.when(delay_of(row) < farthest)
            def _():
                lax.fori_loop(lo, hi, one, 0)

            return carry

        lax.fori_loop(0, z + 1, compute, 0)
        lo, hi = matching(t - farthest)

        def close(r, carry):
            def one(i, carry):
                row = z - i

                @pl.when(delay_of(row) == farthest)
                def _():
                    attend(r, row)

                return carry

            lax.fori_loop(0, z + 1, one, 0)
            settle(r)
            for g, (first, count) in enumerate(GROUPS):
                @pl.when((r >= first) & (r == jnp.minimum(first + count, mine) - 1))
                def _(g=g):
                    share_own(g)
                    if g > 0:
                        share_next(g - 1)
                    if g > 1:
                        share_far(g - 2)

            return carry

        lax.fori_loop(lo, hi, close, 0)
        return carry

    lax.fori_loop(0, farthest + 5 + SKEW[last], wave, 0)
    for g, (first, count) in enumerate(GROUPS):
        @pl.when((mine > first) & (mine <= first + count))
        def _(g=g):
            share_next(g)
            if g > 0:
                share_far(g - 1)
            share_far(g)

    def sent(direction, g, row, columns):
        lo, count = GROUPS[g]
        part = buf.at[lo : lo + count, 0:columns]
        pltpu.make_async_remote_copy(
            src_ref=part, dst_ref=part, send_sem=send.at[direction, g, row],
            recv_sem=recv.at[0, 0], device_id=right, device_id_type=MESH,
        ).wait_send()

    def drain(row, carry):
        upto, rises, _ = route(row)
        for g in range(len(GROUPS)):
            _, up, wrap, down = needs(g, row, upto, rises)
            ring = (z < reach[g]) & (jnp.logical_not(first_core) | (row == z))

            @pl.when(ring)
            def _(g=g):
                sent(0, g, row, 4)
                sent(1, g, row, 3)

            for direction, used in ((2, up), (3, wrap | down)):
                @pl.when(used & first_core)
                def _(g=g, direction=direction):
                    sent(direction, g, row, 8)

            for ahead in (1, 2):
                straight = jnp.logical_not(first_core) & (((z - row) & 1) == 0)

                @pl.when(straight & (z < reach[g]) & (z + ahead < reach[g]))
                def _(g=g, ahead=ahead):
                    sent(1 + ahead, g, row, 1)

        return carry

    lax.fori_loop(0, z + 1, drain, 0)

    for g in range(len(GROUPS)):
        @pl.when(mine > GROUPS[g][0])
        def _(g=g):
            for chip, slot in ((x, 2), (x - 1, 4), (x + 1, 5), (x + 2, 6)):
                share(g, chip, 1 - core, slot, right).wait_recv()
            for slot in range(7):
                share(g, x, core, slot, right).wait_send()


def exchange(plan, collective, bias, meta, queries, keyvals):
    smem = pl.BlockSpec(memory_space=pltpu.SMEM)
    vmem = pl.BlockSpec(memory_space=pltpu.VMEM)
    return pl.pallas_call(
        functools.partial(exchange_kernel, plan),
        name="exchange",
        out_shape=jax.ShapeDtypeStruct((8, SEQS, BLK, BLK), jnp.bfloat16),
        in_specs=[vmem, smem, vmem, vmem],
        out_specs=vmem,
        scratch_shapes=[
            pltpu.VMEM((SEQS, 64, BLK, BLK), jnp.bfloat16),
            pltpu.VMEM((SEQS, 2 * BLK, 2 * BLK), jnp.float32),
            pltpu.VMEM((SEQS, 2 * BLK, 1), jnp.float32),
            pltpu.SemaphoreType.DMA,
            pltpu.SemaphoreType.DMA((len(GROUPS), 64)),
            pltpu.SemaphoreType.DMA((4, len(GROUPS), 8)),
            pltpu.SemaphoreType.DMA((len(GROUPS), 7)),
            pltpu.SemaphoreType.DMA((len(GROUPS), 7)),
        ],
        compiler_params=pltpu.CompilerParams(
            collective_id=collective, has_side_effects=True, vmem_limit_bytes=48 * 1024 * 1024
        ),
    )(bias, meta, queries, keyvals)


def finish_kernel(meta_ref, att_ref, w_ref, out_ref, att_buf, sems):
    first = lax.axis_index("kv") * BLK

    def fetch(r):
        return pltpu.make_async_copy(att_ref.at[:, r], att_buf.at[r], sems.at[r])

    for r in range(SEQS):
        fetch(r).start()
    for r in range(SEQS):
        fetch(r).wait()
        s = meta_ref[0, r]
        live = meta_ref[1, r] > first

        @pl.when(live)
        def _():
            rows = jnp.concatenate([att_buf[r, t] for t in range(8)], axis=1)
            out_ref[s] = jnp.dot(
                rows, w_ref[...], preferred_element_type=jnp.float32
            ).astype(jnp.bfloat16)

        @pl.when(jnp.logical_not(live))
        def _():
            out_ref[s] = jnp.zeros((BLK, 256), jnp.bfloat16)


def finish(meta, attended, w_output):
    vmem = pl.BlockSpec(memory_space=pltpu.VMEM)
    return pl.pallas_call(
        finish_kernel,
        name="finish",
        out_shape=jax.ShapeDtypeStruct((SEQS, BLK, 256), jnp.bfloat16),
        in_specs=[pl.BlockSpec(memory_space=pltpu.SMEM), pl.BlockSpec(memory_space=pl.ANY), vmem],
        out_specs=vmem,
        scratch_shapes=[
            pltpu.VMEM((SEQS, 8, BLK, BLK), jnp.bfloat16),
            pltpu.SemaphoreType.DMA((SEQS,)),
        ],
        compiler_params=pltpu.CompilerParams(vmem_limit_bytes=16 * 1024 * 1024),
    )(meta, attended, w_output)


def per_device(tokens, w_query, w_key, w_value, w_output, chosen, lengths):
    queries, keyvals, bias, meta = project(
        lengths, chosen[:, 0, :], tokens, w_query, w_key, w_value
    )
    attended = lax.cond(
        meta[2, 0] > 0,
        functools.partial(exchange, LIGHT, 0),
        functools.partial(exchange, FULL, 1),
        bias, meta, queries, keyvals,
    )
    return finish(meta, attended, w_output)


def solution(mesh):
    return jax.shard_map(
        per_device,
        mesh=mesh,
        in_specs=(
            P(None, "kv", None),
            P(None, "tp"),
            P(None, "tp"),
            P(None, "tp"),
            P(None, "tp"),
            P(None, "kv", None),
            P(),
        ),
        out_specs=P(None, "kv", "tp"),
        check_vma=False,
    )
```

time: 376 us -> 83.2 us (0.22)
  the two profiles are of different devices: /device:TPU:1 before, /device:TPU:69 now
where the time goes in v2:
time: 83.2 us; the launch traced here: 83 us
  Pallas kernels  81.8 us (98%)
    pallas_call x1, Pallas kernels, exchange(): pl.pallas_call(functools.partial(exchange_kernel, plan), name='exchange',...  73.3 us
    pallas_call x1, Pallas kernels, project(): pl.pallas_call(project_kernel, name='project', out_shape=(jax.ShapeDtypeS...  5.49 us
    pallas_call x1, Pallas kernels, finish(): pl.pallas_call(finish_kernel, name='finish', out_shape=jax.ShapeDtypeStru...  3.06 us

profile of v2, /device:TPU:69, one launch (start us, length us, event | category | flops | bytes accessed | tf_op | source)
XLA Modules:
  0.0 83.0 jit_solution(9064568173674637818)
XLA Ops:
  0.0 5.5 %project.1 = (bf16[8,256,128]{2,1,0:T(8,128)(2,1)S(1)}, bf16[8,128,128]{2,1,0:T(8,128)(2,1)S(1)}, f32[8,8192]{1,0:T(8,128)}, s32[3,8]{1,0:T(4,128)S(1)}) custom-call(s32[8]{0:T(128)} %len_ref.1, s32[8,32]{1,0:T(8,128)} %bitcast.6, bf16[8,128,2048]{2,1,0:T(8,128)(2,1)} %tok_ref.1, bf16[2048,128]{1,0:T(8,128)(2,1)} %wq_ref.1, bf16[64,2048]{1,0:T(8,128)(2,1)} %bitcast.4, ...), custom_call_target="tpu_custom_call" | custom-call | tf_op jit(solution)/shard_map/project/pallas_call | solution.py:96
  5.5 0.5 slice.3
  6.7 0.0 copy-start
  6.7 73.3 %conditional.1 = (bf16[8,8,128,128]{3,2,1,0:T(8,128)(2,1)S(1)}) conditional(s32[]{:T(128)} %bitcast.3, (f32[8,8192]{1,0:T(8,128)}, s32[3,8]{1,0:T(4,128)S(1)}, bf16[8,256,128]{2,1,0:T(8,128)(2,1)S(1)}, bf16[8,128,128]{2,1,0:T(8,128)(2,1)S(1)}) %tuple.11, (f32[8,8192]{1,0:T(8,128)}, s32[3,8]{1,0:T(4,128)S(1)}, bf16[8,256,128]{2,1,0:T(8,128)(2,1)S(1)}, ...), branch_computations={%region_0.0_spmd, %region_1.0_spmd} | conditional | bytes 8 | solution.py:570
  6.7 73.3 %exchange.3 = bf16[8,8,128,128]{3,2,1,0:T(8,128)(2,1)S(1)} custom-call(f32[8,8192]{1,0:T(8,128)} %get-tuple-element.28.bias_ref, s32[3,8]{1,0:T(4,128)S(1)} %get-tuple-element.29.meta_ref, bf16[8,256,128]{2,1,0:T(8,128)(2,1)S(1)} %get-tuple-element.30.q_ref, bf16[8,128,128]{2,1,0:T(8,128)(2,1)S(1)} %get-tuple-element.31.kv_ref), custom_call_target="tpu_custom_call" | custom-call | tf_op jit(solution)/shard_map/cond/branch_1_fun/exchange/pallas_call | solution.py:503
  80.0 0.0 copy-done
  80.0 3.1 %finish.1 = bf16[8,128,256]{2,1,0:T(8,128)(2,1)} custom-call(s32[3,8]{1,0:T(4,128)S(1)} %get-tuple-element.36.meta_ref, bf16[8,8,128,128]{3,2,1,0:T(8,128)(2,1)S(1)} %get-tuple-element.40.att_ref, bf16[1024,256]{1,0:T(8,128)(2,1)S(1)} %copy-done), custom_call_target="tpu_custom_call" | custom-call | tf_op jit(solution)/shard_map/finish/pallas_call | solution.py:552
Async XLA Ops:
  6.7 73.3 %copy-start = (bf16[1024,256]{1,0:T(8,128)(2,1)S(1)}, bf16[1024,256]{1,0:T(8,128)(2,1)}, u32[]{:S(2)}) copy-start(bf16[1024,256]{1,0:T(8,128)(2,1)} %w_ref.1) | copy-start | bytes 1572868

commit v3 on v2

--- a/solution.py
+++ b/solution.py
@@ -15,7 +15,9 @@
 LOG2E = 1.4426950408889634
 NEG = -1e30
 GROUPS = ((0, 2), (2, 2), (4, 1), (5, 3))
-SKEW = (0, 0, 1, 1)
+SKEW = (0, 0, 1, 2)
+SIDE = (1, -1, -1, 1)
+STRAIGHT = (True, True, True, True)
 UPTO = (3, 4, 5, 7, 7, 7, 7, 7)
 FULL = ((8, 8, 7, 5, 4, 3, 3, 2), (8, 7, 4, 3))
 LIGHT = ((8, 8, 5, 4, 2, 2, 2, 1), (8, 4, 3, 2))
@@ -157,7 +159,7 @@
 
     for target in (
         at_kv(z, y + 1), at_kv(z, y - 1),
-        at_tp(x + 1, core), at_tp(x - 1, core), at_tp(x, 1 - core),
+        at_tp(x + 1, core), at_tp(x - 1, core), at_tp(x + 2, core), at_tp(x, 1 - core),
     ):
         greet(target)
     for step in (1, 2, 6, 7):
@@ -171,7 +173,7 @@
     def _():
         greet(at_kv(jnp.int32(2), y))
 
-    pl.semaphore_wait(barrier, jnp.where((z == 2) | (z == 7), 10, 9))
+    pl.semaphore_wait(barrier, jnp.where((z == 2) | (z == 7), 11, 10))
     own.wait()
 
     def link(g, c, sem, target):
@@ -182,11 +184,11 @@
             device_id=target, device_id_type=MESH,
         )
 
-    def to_right(g, c, row):
-        link(g, c, send.at[0, g, row], at_kv(z, y + 1)).start()
-
-    def to_left(g, c, row):
-        link(g, c, send.at[1, g, row], at_kv(z, y - 1)).start()
+    def to_long(g, c, row, side):
+        link(g, c, send.at[0, g, row], at_kv(z, y + side)).start()
+
+    def to_short(g, c, row, side):
+        link(g, c, send.at[1, g, row], at_kv(z, y - side)).start()
 
     def arrived(g, c):
         link(g, c, send.at[0, 0, 0], at_kv(z, y + 1)).wait_recv()
@@ -221,12 +223,13 @@
     def row_items(u, row, upto, rises):
         for g in range(len(GROUPS)):
             step = u - SKEW[g]
+            side = SIDE[g]
             takes, up, wrap, down = needs(g, row, upto, rises)
             in_row = row == z
 
             @pl.when((step >= 0) & (step < 5) & takes)
-            def _(g=g, step=step, up=up, wrap=wrap, down=down, in_row=in_row):
-                c = row * 8 + ((y - step) & 7)
+            def _(g=g, step=step, side=side, up=up, wrap=wrap, down=down, in_row=in_row):
+                c = row * 8 + ((y - side * step) & 7)
 
                 @pl.when(jnp.logical_not(in_row & (step == 0)))
                 def _():
@@ -234,22 +237,22 @@
 
                 @pl.when(in_row & (step < 4))
                 def _():
-                    to_right(g, c, row)
+                    to_long(g, c, row, side)
 
                 @pl.when(in_row & (step == 0))
                 def _():
-                    to_left(g, c, row)
+                    to_short(g, c, row, side)
 
                 column(g, c, row, up, wrap, down)
 
                 @pl.when((step > 0) & (step < 4))
                 def _():
-                    c = row * 8 + ((y + step) & 7)
+                    c = row * 8 + ((y + side * step) & 7)
                     arrived(g, c)
 
                     @pl.when(in_row & (step < 3))
                     def _():
-                        to_left(g, c, row)
+                        to_short(g, c, row, side)
 
                     column(g, c, row, up, wrap, down)
 
@@ -259,17 +262,18 @@
         for g in range(len(GROUPS)):
             step = t - far - SKEW[g]
             used = z < reach[g]
+            side = SIDE[g] * (1 - 2 * (row & 1))
 
             @pl.when((step == 0) & used)
-            def _(g=g):
+            def _(g=g, side=side):
                 c = row * 8 + y
 
                 @pl.when(row != z)
                 def _():
                     arrived(g, c)
 
-                to_right(g, c, row)
-                to_left(g, c, row)
+                to_long(g, c, row, side)
+                to_short(g, c, row, side)
 
                 for ahead in (1, 2):
                     @pl.when(((away & 1) == 0) & (z + ahead < reach[g]))
@@ -277,59 +281,62 @@
                         link(g, c, send.at[1 + ahead, g, row], at_kv(z + ahead, y)).start()
 
             @pl.when((step > 0) & (step < 5) & used)
-            def _(g=g, step=step):
-                c = row * 8 + ((y - step) & 7)
+            def _(g=g, step=step, side=side):
+                c = row * 8 + ((y - side * step) & 7)
                 arrived(g, c)
 
                 @pl.when(step < 4)
                 def _():
-                    to_right(g, c, row)
-                    c2 = row * 8 + ((y + step) & 7)
+                    to_long(g, c, row, side)
+                    c2 = row * 8 + ((y + side * step) & 7)
                     arrived(g, c2)
 
                     @pl.when(step < 3)
                     def _():
-                        to_left(g, c2, row)
+                        to_short(g, c2, row, side)
 
     scale = HD ** (-0.5) * LOG2E
-    row_at = lax.broadcasted_iota(jnp.int32, (2 * BLK, BLK), 0) & (BLK - 1)
-    col_at = lax.broadcasted_iota(jnp.int32, (2 * BLK, BLK), 1)
     ones = jnp.ones((8 * BLK, BLK), jnp.bfloat16)
     lane = lax.broadcasted_iota(jnp.int32, (BLK, BLK), 1)
     sub = lax.broadcasted_iota(jnp.int32, (BLK, BLK), 0)
 
-    def scores(r, row):
-        keys = buf[r, pl.ds(row * 8, 8)].reshape(8 * BLK, BLK)
+    def scores(r, row, rows, keys):
         raw = lax.dot_general(
-            q_ref[r], keys, (((1,), (1,)), ((), ())), preferred_element_type=jnp.float32
+            q_ref[r, rows], keys, (((1,), (1,)), ((), ())), preferred_element_type=jnp.float32
         )
         bias = bias_ref[pl.ds(r, 1), pl.ds(pl.multiple_of(row * 8 * BLK, 8 * BLK), 8 * BLK)]
-        return raw * scale + bias, jnp.concatenate([keys, ones], axis=1)
+        return raw * scale + bias
 
     def attend(r, row):
         @pl.when(row == z)
         def _():
-            s, wide = scores(r, row)
-            parts = []
-            for i in range(8):
-                part = s[:, i * BLK : (i + 1) * BLK]
-                parts.append(jnp.where((col_at <= row_at) | (y != i), part, NEG))
-            s = jnp.concatenate(parts, axis=1)
-            best = jnp.max(s, axis=1, keepdims=True)
-            p = jnp.exp2(s - best).astype(jnp.bfloat16)
-            top[r] = best
-            acc[r] = jnp.dot(p, wide, preferred_element_type=jnp.float32)
+            keys = buf[r, pl.ds(row * 8, 8)].reshape(8 * BLK, BLK)
+            wide = jnp.concatenate([keys, ones], axis=1)
+            for rows in (slice(0, BLK), slice(BLK, 2 * BLK)):
+                s = scores(r, row, rows, keys)
+                parts = []
+                for i in range(8):
+                    part = s[:, i * BLK : (i + 1) * BLK]
+                    parts.append(jnp.where((lane <= sub) | (y != i), part, NEG))
+                s = jnp.concatenate(parts, axis=1)
+                best = jnp.max(s, axis=1, keepdims=True)
+                p = jnp.exp2(s - best).astype(jnp.bfloat16)
+                top[r, rows] = best
+                acc[r, rows] = jnp.dot(p, wide, preferred_element_type=jnp.float32)
 
         @pl.when(row != z)
         def _():
-            s, wide = scores(r, row)
-            old = top[r]
-            best = jnp.maximum(old, jnp.max(s, axis=1, keepdims=True))
-            p = jnp.exp2(s - best).astype(jnp.bfloat16)
-            top[r] = best
-            acc[r] = acc[r] * jnp.exp2(old - best) + jnp.dot(
-                p, wide, preferred_element_type=jnp.float32
-            )
+            keys = buf[r, pl.ds(row * 8, 8)].reshape(8 * BLK, BLK)
+            wide = jnp.concatenate([keys, ones], axis=1)
+            for rows in (slice(0, BLK), slice(BLK, 2 * BLK)):
+                s = scores(r, row, rows, keys)
+                old = top[r, rows]
+                best = jnp.maximum(old, jnp.max(s, axis=1, keepdims=True))
+                p = jnp.exp2(s - best).astype(jnp.bfloat16)
+                top[r, rows] = best
+                acc[r, rows] = acc[r, rows] * jnp.exp2(old - best) + jnp.dot(
+                    p, wide, preferred_element_type=jnp.float32
+                )
 
     def settle(r):
         total = acc[r]
@@ -353,14 +360,16 @@
         share(g, x, core, 0, right).start()
         share(g, x, core, 1, left).start()
         share(g, x, core, 2, sibling).start()
+        if STRAIGHT[g]:
+            share(g, x, core, 3, at_tp(x + 2, core)).start()
 
     def share_next(g):
         share(g, x - 1, core, 0, right).wait_recv()
-        if g % 2 == 0:
+        if g % 2 == 0 and not STRAIGHT[g]:
             share(g, x - 1, core, 3, right).start()
         share(g, x - 1, core, 4, sibling).start()
         share(g, x + 1, core, 1, right).wait_recv()
-        if g % 2 == 1:
+        if g % 2 == 1 and not STRAIGHT[g]:
             share(g, x + 1, core, 3, left).start()
         share(g, x + 1, core, 5, sibling).start()
 
@@ -522,29 +531,23 @@
     )(bias, meta, queries, keyvals)
 
 
-def finish_kernel(meta_ref, att_ref, w_ref, out_ref, att_buf, sems):
+def finish_kernel(meta_ref, att_ref, w_ref, out_ref):
     first = lax.axis_index("kv") * BLK
-
-    def fetch(r):
-        return pltpu.make_async_copy(att_ref.at[:, r], att_buf.at[r], sems.at[r])
-
-    for r in range(SEQS):
-        fetch(r).start()
-    for r in range(SEQS):
-        fetch(r).wait()
-        s = meta_ref[0, r]
-        live = meta_ref[1, r] > first
-
-        @pl.when(live)
-        def _():
-            rows = jnp.concatenate([att_buf[r, t] for t in range(8)], axis=1)
-            out_ref[s] = jnp.dot(
-                rows, w_ref[...], preferred_element_type=jnp.float32
-            ).astype(jnp.bfloat16)
-
-        @pl.when(jnp.logical_not(live))
-        def _():
-            out_ref[s] = jnp.zeros((BLK, 256), jnp.bfloat16)
+    for r in range(0, SEQS, 2):
+        @pl.when(meta_ref[1, r] > first)
+        def _(r=r):
+            rows = jnp.concatenate(
+                [att_ref[t, r : r + 2].reshape(2 * BLK, BLK) for t in range(8)], axis=1
+            )
+            mixed = jnp.dot(rows, w_ref[...], preferred_element_type=jnp.float32)
+            out_ref[meta_ref[0, r]] = mixed[:BLK].astype(jnp.bfloat16)
+            kept = jnp.where(meta_ref[1, r + 1] > first, mixed[BLK:], 0.0)
+            out_ref[meta_ref[0, r + 1]] = kept.astype(jnp.bfloat16)
+
+        @pl.when(meta_ref[1, r] <= first)
+        def _(r=r):
+            for i in (r, r + 1):
+                out_ref[meta_ref[0, i]] = jnp.zeros((BLK, 256), jnp.bfloat16)
 
 
 def finish(meta, attended, w_output):
@@ -553,12 +556,8 @@
         finish_kernel,
         name="finish",
         out_shape=jax.ShapeDtypeStruct((SEQS, BLK, 256), jnp.bfloat16),
-        in_specs=[pl.BlockSpec(memory_space=pltpu.SMEM), pl.BlockSpec(memory_space=pl.ANY), vmem],
+        in_specs=[pl.BlockSpec(memory_space=pltpu.SMEM), vmem, vmem],
         out_specs=vmem,
-        scratch_shapes=[
-            pltpu.VMEM((SEQS, 8, BLK, BLK), jnp.bfloat16),
-            pltpu.SemaphoreType.DMA((SEQS,)),
-        ],
         compiler_params=pltpu.CompilerParams(vmem_limit_bytes=16 * 1024 * 1024),
     )(meta, attended, w_output)
 

time: 83.2 us -> 75.6 us (0.909)
  the two profiles are of different devices: /device:TPU:69 before, /device:TPU:193 now
where the time goes in v3:
time: 75.6 us; the launch traced here: 75.5 us
  Pallas kernels  74.3 us (98%)
    pallas_call x1, Pallas kernels, exchange(): pl.pallas_call(functools.partial(exchange_kernel, plan), name='exchange',...  68 us
    pallas_call x1, Pallas kernels, project(): pl.pallas_call(project_kernel, name='project', out_shape=(jax.ShapeDtypeS...  4.53 us
    pallas_call x1, Pallas kernels, finish(): pl.pallas_call(finish_kernel, name='finish', out_shape=jax.ShapeDtypeStru...  1.75 us

profile of v3, /device:TPU:193, one launch (start us, length us, event | category | flops | bytes accessed | tf_op | source)
XLA Modules:
  0.0 75.5 jit_solution(8658585942803570396)
XLA Ops:
  0.0 4.5 %project.1 = (bf16[8,256,128]{2,1,0:T(8,128)(2,1)S(1)}, bf16[8,128,128]{2,1,0:T(8,128)(2,1)S(1)}, f32[8,8192]{1,0:T(8,128)}, s32[3,8]{1,0:T(4,128)S(1)}) custom-call(s32[8]{0:T(128)} %len_ref.1, s32[8,32]{1,0:T(8,128)} %bitcast.6, bf16[8,128,2048]{2,1,0:T(8,128)(2,1)} %tok_ref.1, bf16[2048,128]{1,0:T(8,128)(2,1)} %wq_ref.1, bf16[64,2048]{1,0:T(8,128)(2,1)} %bitcast.4, ...), custom_call_target="tpu_custom_call" | custom-call | tf_op jit(solution)/shard_map/project/pallas_call | solution.py:98
  4.5 0.5 slice.3
  5.7 0.0 copy-start
  5.7 68.0 %conditional.1 = (bf16[8,8,128,128]{3,2,1,0:T(8,128)(2,1)S(1)}) conditional(s32[]{:T(128)} %bitcast.3, (f32[8,8192]{1,0:T(8,128)}, s32[3,8]{1,0:T(4,128)S(1)}, bf16[8,256,128]{2,1,0:T(8,128)(2,1)S(1)}, bf16[8,128,128]{2,1,0:T(8,128)(2,1)S(1)}) %tuple.11, (f32[8,8192]{1,0:T(8,128)}, s32[3,8]{1,0:T(4,128)S(1)}, bf16[8,256,128]{2,1,0:T(8,128)(2,1)S(1)}, ...), branch_computations={%region_0.0_spmd, %region_1.0_spmd} | conditional | bytes 8 | solution.py:569
  5.7 68.0 %exchange.3 = bf16[8,8,128,128]{3,2,1,0:T(8,128)(2,1)S(1)} custom-call(f32[8,8192]{1,0:T(8,128)} %get-tuple-element.28.bias_ref, s32[3,8]{1,0:T(4,128)S(1)} %get-tuple-element.29.meta_ref, bf16[8,256,128]{2,1,0:T(8,128)(2,1)S(1)} %get-tuple-element.30.q_ref, bf16[8,128,128]{2,1,0:T(8,128)(2,1)S(1)} %get-tuple-element.31.kv_ref), custom_call_target="tpu_custom_call" | custom-call | tf_op jit(solution)/shard_map/cond/branch_1_fun/exchange/pallas_call | solution.py:512
  73.7 0.0 copy-done
  73.7 1.8 %finish.1 = bf16[8,128,256]{2,1,0:T(8,128)(2,1)} custom-call(s32[3,8]{1,0:T(4,128)S(1)} %get-tuple-element.36.meta_ref, bf16[8,8,128,128]{3,2,1,0:T(8,128)(2,1)S(1)} %get-tuple-element.40.att_ref, bf16[1024,256]{1,0:T(8,128)(2,1)S(1)} %copy-done), custom_call_target="tpu_custom_call" | custom-call | tf_op jit(solution)/shard_map/finish/pallas_call | solution.py:555
Async XLA Ops:
  5.7 68.0 %copy-start = (bf16[1024,256]{1,0:T(8,128)(2,1)S(1)}, bf16[1024,256]{1,0:T(8,128)(2,1)}, u32[]{:S(2)}) copy-start(bf16[1024,256]{1,0:T(8,128)(2,1)} %w_ref.1) | copy-start | bytes 1572868

commit v4 on v3

--- a/solution.py
+++ b/solution.py
@@ -15,7 +15,7 @@
 LOG2E = 1.4426950408889634
 NEG = -1e30
 GROUPS = ((0, 2), (2, 2), (4, 1), (5, 3))
-SKEW = (0, 0, 1, 2)
+SKEW = (0, 0, 2, 2)
 SIDE = (1, -1, -1, 1)
 STRAIGHT = (True, True, True, True)
 UPTO = (3, 4, 5, 7, 7, 7, 7, 7)
@@ -137,6 +137,11 @@
     ranks, reach = plan
     ranks_at, upto_at = nibble(ranks), nibble(UPTO)
     hops_max_at = nibble([max(hop_count(at, row) for row in range(at + 1)) for at in range(8)])
+    deepest = [
+        7 if any(UPTO[row] + 1 < reach[g] for row in range(8)) else reach[g] - 1
+        for g in range(len(GROUPS))
+    ]
+    skew_max_at = nibble([max(SKEW[g] for g in range(len(GROUPS)) if at <= deepest[g]) for at in range(8)])
     block = lax.axis_index("kv")
     member = lax.axis_index("tp")
     z, y = block >> 3, block & 7
@@ -222,78 +227,82 @@
 
     def row_items(u, row, upto, rises):
         for g in range(len(GROUPS)):
-            step = u - SKEW[g]
-            side = SIDE[g]
-            takes, up, wrap, down = needs(g, row, upto, rises)
-            in_row = row == z
-
-            @pl.when((step >= 0) & (step < 5) & takes)
-            def _(g=g, step=step, side=side, up=up, wrap=wrap, down=down, in_row=in_row):
-                c = row * 8 + ((y - side * step) & 7)
-
-                @pl.when(jnp.logical_not(in_row & (step == 0)))
-                def _():
-                    arrived(g, c)
-
-                @pl.when(in_row & (step < 4))
-                def _():
-                    to_long(g, c, row, side)
-
-                @pl.when(in_row & (step == 0))
-                def _():
-                    to_short(g, c, row, side)
-
-                column(g, c, row, up, wrap, down)
-
-                @pl.when((step > 0) & (step < 4))
-                def _():
-                    c = row * 8 + ((y + side * step) & 7)
-                    arrived(g, c)
-
-                    @pl.when(in_row & (step < 3))
+            @pl.when(z <= deepest[g])
+            def _(g=g):
+                step = u - SKEW[g]
+                side = SIDE[g]
+                takes, up, wrap, down = needs(g, row, upto, rises)
+                in_row = row == z
+
+                @pl.when((step >= 0) & (step < 5) & takes)
+                def _(g=g, step=step, side=side, up=up, wrap=wrap, down=down, in_row=in_row):
+                    c = row * 8 + ((y - side * step) & 7)
+
+                    @pl.when(jnp.logical_not(in_row & (step == 0)))
+                    def _():
+                        arrived(g, c)
+
+                    @pl.when(in_row & (step < 4))
+                    def _():
+                        to_long(g, c, row, side)
+
+                    @pl.when(in_row & (step == 0))
                     def _():
                         to_short(g, c, row, side)
 
                     column(g, c, row, up, wrap, down)
+
+                    @pl.when((step > 0) & (step < 4))
+                    def _():
+                        c = row * 8 + ((y + side * step) & 7)
+                        arrived(g, c)
+
+                        @pl.when(in_row & (step < 3))
+                        def _():
+                            to_short(g, c, row, side)
+
+                        column(g, c, row, up, wrap, down)
 
     def column_items(t, row):
         away = z - row
         far = (away + 1) >> 1
         for g in range(len(GROUPS)):
-            step = t - far - SKEW[g]
-            used = z < reach[g]
-            side = SIDE[g] * (1 - 2 * (row & 1))
-
-            @pl.when((step == 0) & used)
-            def _(g=g, side=side):
-                c = row * 8 + y
-
-                @pl.when(row != z)
-                def _():
+            @pl.when(z <= deepest[g])
+            def _(g=g):
+                step = t - far - SKEW[g]
+                used = z < reach[g]
+                side = SIDE[g] * (1 - 2 * (row & 1))
+
+                @pl.when((step == 0) & used)
+                def _(g=g, side=side):
+                    c = row * 8 + y
+
+                    @pl.when(row != z)
+                    def _():
+                        arrived(g, c)
+
+                    to_long(g, c, row, side)
+                    to_short(g, c, row, side)
+
+                    for ahead in (1, 2):
+                        @pl.when(((away & 1) == 0) & (z + ahead < reach[g]))
+                        def _(ahead=ahead):
+                            link(g, c, send.at[1 + ahead, g, row], at_kv(z + ahead, y)).start()
+
+                @pl.when((step > 0) & (step < 5) & used)
+                def _(g=g, step=step, side=side):
+                    c = row * 8 + ((y - side * step) & 7)
                     arrived(g, c)
 
-                to_long(g, c, row, side)
-                to_short(g, c, row, side)
-
-                for ahead in (1, 2):
-                    @pl.when(((away & 1) == 0) & (z + ahead < reach[g]))
-                    def _(ahead=ahead):
-                        link(g, c, send.at[1 + ahead, g, row], at_kv(z + ahead, y)).start()
-
-            @pl.when((step > 0) & (step < 5) & used)
-            def _(g=g, step=step, side=side):
-                c = row * 8 + ((y - side * step) & 7)
-                arrived(g, c)
-
-                @pl.when(step < 4)
-                def _():
-                    to_long(g, c, row, side)
-                    c2 = row * 8 + ((y + side * step) & 7)
-                    arrived(g, c2)
-
-                    @pl.when(step < 3)
+                    @pl.when(step < 4)
                     def _():
-                        to_short(g, c2, row, side)
+                        to_long(g, c, row, side)
+                        c2 = row * 8 + ((y + side * step) & 7)
+                        arrived(g, c2)
+
+                        @pl.when(step < 3)
+                        def _():
+                            to_short(g, c2, row, side)
 
     scale = HD ** (-0.5) * LOG2E
     ones = jnp.ones((8 * BLK, BLK), jnp.bfloat16)
@@ -379,6 +388,7 @@
 
     last = len(GROUPS) - 1
     farthest = jnp.where(first_core, hops_max_at(z), (z + 1) >> 1)
+    skew_max = skew_max_at(z)
 
     def delay_of(row):
         return jnp.where(first_core, route(row)[2], (z - row + 1) >> 1)
@@ -386,15 +396,17 @@
 
     def wave(t, carry):
         def comm(i, carry):
-            row = z - i
+            row = jnp.where((z == 2) | (z == 3), i, z - i)
             upto, rises, hops = route(row)
             u = t - hops
 
-            @pl.when(first_core)
+            @pl.when(first_core & (u >= 0) & (u <= 4 + skew_max))
             def _():
                 row_items(u, row, upto, rises)
 
-            @pl.when(jnp.logical_not(first_core))
+            since = t - ((z - row + 1) >> 1)
+
+            @pl.when(jnp.logical_not(first_core) & (since >= 0) & (since <= 4 + skew_max))
             def _():
                 column_items(t, row)
 
@@ -412,14 +424,16 @@
 
         def compute(i, carry):
             row = z - i
-            lo, hi = matching(t - delay_of(row))
+            delay = delay_of(row)
+            since = t - delay - 4
 
             def one(r, carry):
                 attend(r, row)
                 return carry
 
-            @pl.when(delay_of(row) < farthest)
+            @pl.when((delay < farthest) & (since >= 0) & (since <= skew_max))
             def _():
+                lo, hi = matching(t - delay)
                 lax.fori_loop(lo, hi, one, 0)
 
             return carry
@@ -453,7 +467,7 @@
         lax.fori_loop(lo, hi, close, 0)
         return carry
 
-    lax.fori_loop(0, farthest + 5 + SKEW[last], wave, 0)
+    lax.fori_loop(0, farthest + 5 + skew_max, wave, 0)
     for g, (first, count) in enumerate(GROUPS):
         @pl.when((mine > first) & (mine <= first + count))
         def _(g=g):

time: 75.6 us -> 76.4 us (1.011)
  Pallas kernels: 74.3 us -> 75.1 us
where the time goes in v4:
time: 76.4 us
  Pallas kernels  75.1 us (98%)
    pallas_call x1, Pallas kernels, exchange(): pl.pallas_call(functools.partial(exchange_kernel, plan), name='exchange',...  68.1 us
    pallas_call x1, Pallas kernels, project(): pl.pallas_call(project_kernel, name='project', out_shape=(jax.ShapeDtypeS...  5.01 us
    pallas_call x1, Pallas kernels, finish(): pl.pallas_call(finish_kernel, name='finish', out_shape=jax.ShapeDtypeStru...  2.04 us

profile of v4, /device:TPU:193, one launch (start us, length us, event | category | flops | bytes accessed | tf_op | source)
XLA Modules:
  0.0 76.4 jit_solution(7654186440975849529)
XLA Ops:
  0.0 5.0 %project.1 = (bf16[8,256,128]{2,1,0:T(8,128)(2,1)S(1)}, bf16[8,128,128]{2,1,0:T(8,128)(2,1)S(1)}, f32[8,8192]{1,0:T(8,128)}, s32[3,8]{1,0:T(4,128)S(1)}) custom-call(s32[8]{0:T(128)} %len_ref.1, s32[8,32]{1,0:T(8,128)} %bitcast.6, bf16[8,128,2048]{2,1,0:T(8,128)(2,1)} %tok_ref.1, bf16[2048,128]{1,0:T(8,128)(2,1)} %wq_ref.1, bf16[64,2048]{1,0:T(8,128)(2,1)} %bitcast.4, ...), custom_call_target="tpu_custom_call" | custom-call | tf_op jit(solution)/shard_map/project/pallas_call | solution.py:98
  5.0 0.5 slice.3
  6.2 0.0 copy-start
  6.2 68.1 %conditional.1 = (bf16[8,8,128,128]{3,2,1,0:T(8,128)(2,1)S(1)}) conditional(s32[]{:T(128)} %bitcast.3, (f32[8,8192]{1,0:T(8,128)}, s32[3,8]{1,0:T(4,128)S(1)}, bf16[8,256,128]{2,1,0:T(8,128)(2,1)S(1)}, bf16[8,128,128]{2,1,0:T(8,128)(2,1)S(1)}) %tuple.11, (f32[8,8192]{1,0:T(8,128)}, s32[3,8]{1,0:T(4,128)S(1)}, bf16[8,256,128]{2,1,0:T(8,128)(2,1)S(1)}, ...), branch_computations={%region_0.0_spmd, %region_1.0_spmd} | conditional | bytes 8 | solution.py:583
  6.2 68.1 %exchange.3 = bf16[8,8,128,128]{3,2,1,0:T(8,128)(2,1)S(1)} custom-call(f32[8,8192]{1,0:T(8,128)} %get-tuple-element.28.bias_ref, s32[3,8]{1,0:T(4,128)S(1)} %get-tuple-element.29.meta_ref, bf16[8,256,128]{2,1,0:T(8,128)(2,1)S(1)} %get-tuple-element.30.q_ref, bf16[8,128,128]{2,1,0:T(8,128)(2,1)S(1)} %get-tuple-element.31.kv_ref), custom_call_target="tpu_custom_call" | custom-call | tf_op jit(solution)/shard_map/cond/branch_1_fun/exchange/pallas_call | solution.py:526
  74.3 0.0 copy-done
  74.3 2.0 %finish.1 = bf16[8,128,256]{2,1,0:T(8,128)(2,1)} custom-call(s32[3,8]{1,0:T(4,128)S(1)} %get-tuple-element.36.meta_ref, bf16[8,8,128,128]{3,2,1,0:T(8,128)(2,1)S(1)} %get-tuple-element.40.att_ref, bf16[1024,256]{1,0:T(8,128)(2,1)S(1)} %copy-done), custom_call_target="tpu_custom_call" | custom-call | tf_op jit(solution)/shard_map/finish/pallas_call | solution.py:569
Async XLA Ops:
  6.2 68.1 %copy-start = (bf16[1024,256]{1,0:T(8,128)(2,1)S(1)}, bf16[1024,256]{1,0:T(8,128)(2,1)}, u32[]{:S(2)}) copy-start(bf16[1024,256]{1,0:T(8,128)(2,1)} %w_ref.1) | copy-start | bytes 1572868
